TPU v7x, 32 devices: a whole 2x2x4 slice. The times are simulated.
32 devices in a mesh: sp: 8 (over z, y), tp: 4 (over x, core).
Axes of the slice: x: 2, y: 2, z: 4, core: 2. Of those that a mesh axis runs over, the one named last changes fastest.
Arguments:
- target: bfloat16 [56, 2048], P('sp'), may hold values from -6 to 6
- source: bfloat16 [2048, 2048], P('sp'), may hold values from -6 to 6
- tgt_gain: float32 [2, 2048], replicated, may hold values from 0.1 to 1.9
- src_gain: float32 [2, 2048], replicated, may hold values from 0.1 to 1.9
- w_query: bfloat16 [2, 2048, 2048], P(None, None, 'tp'), may hold values from -0.125 to 0.125
- w_key: bfloat16 [2, 2048, 2048], P(None, None, 'tp'), may hold values from -0.125 to 0.125
- w_value: bfloat16 [2, 2048, 2048], P(None, None, 'tp'), may hold values from -0.125 to 0.125
- w_out: bfloat16 [2, 2048, 2048], P(None, 'tp'), may hold values from -0.125 to 0.125
- score_scale: float32 [2, 8], P(None, 'tp'), may hold values from 1.5 to 4
Outputs:
- result: bfloat16 [56, 2048], P('sp')
All inputs are finite; a program needn't handle non-finite values.
Results may differ from a plain program's by a relative error of at most 0.015.
Values may be sent and summed in bfloat16 or wider, within the bound.
A program may use at most 64 MiB of HBM per device.

v0:
```python
import math
import jax
import jax.numpy as jnp
from jax import lax
from jax.sharding import PartitionSpec as P

HEAD_DIM = 256
EPS = 1e-06


def row_scale(values):
    return lax.rsqrt(jnp.mean(values * values, axis=-1, keepdims=True) + EPS)


def head_norm(projected):
    heads = projected.reshape(projected.shape[0], -1, HEAD_DIM)
    heads = heads * row_scale(heads)
    return heads.reshape(projected.shape).astype(jnp.bfloat16)


def source_side(src_float, src_scale, gain_row, key_weight, value_weight):
    normed_src = (src_float * src_scale * gain_row).astype(jnp.bfloat16)
    key_rows = head_norm(jnp.dot(normed_src, key_weight, preferred_element_type=jnp.float32))
    value_rows = jnp.dot(normed_src, value_weight, preferred_element_type=jnp.float32).astype(
        jnp.bfloat16
    )
    return (key_rows, value_rows)


def attend(queries, key_rows, value_rows, scales):
    root = math.sqrt(HEAD_DIM)
    count = queries.shape[0]
    local_heads = scales.shape[0]
    query_heads = queries.reshape(count, local_heads, HEAD_DIM)
    key_heads = key_rows.reshape(key_rows.shape[0], local_heads, HEAD_DIM)
    value_heads = value_rows.reshape(value_rows.shape[0], local_heads, HEAD_DIM)
    scores = jnp.einsum("qhd,khd->hqk", query_heads, key_heads, preferred_element_type=jnp.float32)
    logits = scales[:, None, None] * (scores / root - root)
    weights = jnp.exp(logits)
    denominators = jnp.sum(weights, axis=2).T
    numerators = jnp.einsum(
        "hqk,khd->qhd",
        weights.astype(jnp.bfloat16),
        value_heads,
        preferred_element_type=jnp.float32,
    )
    return (numerators.reshape(count, local_heads * HEAD_DIM), denominators)


def place(terms):
    numer_all = terms[0]
    denom_all = terms[1]
    return (numer_all, denom_all)


def body(target, source, tgt_gain, src_gain, w_query, w_key, w_value, w_out, score_scale):
    local_heads = w_query.shape[2] // HEAD_DIM
    width = local_heads * HEAD_DIM
    tok_rows = target.shape[0]
    layer_count = w_query.shape[0]
    src_float = source.astype(jnp.float32)
    src_scale = row_scale(src_float)
    hidden = target
    for layer_index in range(layer_count):
        key_rows, value_rows = source_side(
            src_float, src_scale, src_gain[layer_index], w_key[layer_index], w_value[layer_index]
        )
        scales = score_scale[layer_index]
        hidden_float = hidden.astype(jnp.float32)
        normed_tgt = (hidden_float * row_scale(hidden_float) * tgt_gain[layer_index]).astype(
            jnp.bfloat16
        )
        weight_now = w_query[layer_index]
        query_rows = head_norm(jnp.dot(normed_tgt, weight_now, preferred_element_type=jnp.float32))
        running = place(
            attend(
                lax.all_gather(query_rows, "sp", axis=0, tiled=True), key_rows, value_rows, scales
            )
        )
        numerators, denominators = (
            lax.psum_scatter(running[0], "sp", scatter_dimension=0, tiled=True),
            lax.psum_scatter(running[1], "sp", scatter_dimension=0, tiled=True),
        )
        attended = (
            (numerators.reshape(tok_rows, local_heads, HEAD_DIM) / denominators[:, :, None])
            .reshape(tok_rows, width)
            .astype(jnp.bfloat16)
        )
        share = jnp.dot(attended, w_out[layer_index], preferred_element_type=jnp.float32).astype(
            jnp.bfloat16
        )
        branch = lax.psum(share.astype(jnp.float32).astype(jnp.bfloat16), "tp").astype(jnp.float32)
        hidden = (hidden_float + branch).astype(jnp.bfloat16)
    return hidden


def solution(mesh):
    placed = (
        P("sp", None),
        P("sp", None),
        P(),
        P(),
        P(None, None, "tp"),
        P(None, None, "tp"),
        P(None, None, "tp"),
        P(None, "tp", None),
        P(None, "tp"),
    )
    return jax.shard_map(body, mesh=mesh, in_specs=placed, out_specs=P("sp", None), check_vma=False)
```

profile of v0, /device:TPU:0, one launch (start us, length us, event | category | flops | bytes accessed | tf_op | source)
XLA Modules:
  0.0 235.5 jit_solution(8419340724434277195)
XLA Ops:
  0.0 1.5 fusion.6
  1.5 0.8 fusion.73
  2.3 3.8 %slice_bitcast_fusion.2 = (bf16[512,2048]{0,1:T(8,128)(2,1)S(1)}, bf16[512,2048]{0,1:T(8,128)(2,1)}) fusion(bf16[2,2048,512]{2,1,0:T(8,128)(2,1)} %param.14), kind=kLoop, calls=%fused_computation.20 | loop fusion | bytes 8388608 | tf_op jit(solution)/shard_map/dot_general | solution.py:23
  6.2 0.0 copy-start.3
  6.2 2.5 %copy.31 = bf16[512,2048]{1,0:T(8,128)(2,1)} copy(bf16[512,2048]{0,1:T(8,128)(2,1)S(1)} %get-tuple-element.7) | data formatting | bytes 4194304 | tf_op jit(solution)/shard_map/dot_general | solution.py:23
  8.6 0.0 copy-done.3
  8.6 0.0 copy-start.1
  8.6 3.4 %multiply_reduce_fusion.1 = (f32[256,2]{0,1:T(2,128)S(1)}, f32[256,2,256]{0,2,1:T(8,128)}) fusion(bf16[2,256,2048]{2,1,0:T(8,128)(2,1)} %bitcast.104, f32[2048]{0:T(1024)S(1)} %bitcast.117, f32[256]{0:T(256)S(1)} %add_rsqrt_fusion.4, bf16[256,2048]{1,0:T(8,128)(2,1)S(1)} %copy-done.3), kind=kOutput, calls=%fused_computation.42 | convolution fusion | flops 539229696 | bytes 3681280 | tf_op jit(solution)/shard_map/dot_general | solution.py:23
  12.0 0.0 copy-done.1
  12.0 2.3 slice_bitcast_fusion.3
  14.3 0.0 copy-start.7
  14.3 0.0 copy-start.4
  14.3 2.9 %copy.30 = bf16[512,2048]{1,0:T(8,128)(2,1)S(1)} copy(bf16[512,2048]{0,1:T(8,128)(2,1)} %get-tuple-element.5) | data formatting | bytes 4194304 | tf_op jit(solution)/shard_map/dot_general | solution.py:74
  17.3 0.0 copy-done.7
  17.3 0.0 copy-start.9
  17.3 0.0 copy-done.4
  17.3 0.1 fusion.43
  17.5 0.7 multiply_reduce_fusion.3
  18.2 0.1 multiply_convert_fusion.5
  18.3 32.4 %all-gather = bf16[8,7,512]{2,1,0:T(8,128)(2,1)S(1)} all-gather(bf16[1,7,512]{2,1,0:T(8,128)(2,1)S(1)} %bitcast.113), channel_id=1, replica_groups=mesh['sp'=8,'tp'=4] {'sp'}, dimensions={0}, use_global_device_ids=true | all-gather | bytes 64512 | tf_op jit(solution)/shard_map/all_gather | solution.py:77
  50.7 0.0 copy-done.9
  50.7 0.0 copy-start.6
  50.7 0.0 copy-start.8
  50.7 0.0 copy-start
  50.7 2.5 %fusion.17 = bf16[256,512]{1,0:T(8,128)(2,1)S(1)} fusion(bf16[2,2048,512]{2,1,0:T(8,128)(2,1)} %param.15, bf16[256,2048]{1,0:T(8,128)(2,1)S(1)} %copy-done.3, f32[2048]{0:T(1024)S(1)} %bitcast.118, f32[256]{0:T(256)S(1)} %add_rsqrt_fusion.4), kind=kOutput, calls=%fused_computation.23 | convolution fusion | flops 539099136 | bytes 3417088 | tf_op jit(solution)/shard_map/dot_general | solution.py:24
  53.2 0.0 copy-done.6
  53.2 0.3 fusion.75
  53.5 0.2 convolution_bitcast_fusion.1
  53.7 22.6 %fusion = f32[8,512]{1,0:T(8,128)S(1)} fusion(f32[56,512]{1,0:T(8,128)S(1)} %bitcast.105), kind=kCustom, calls=%all-reduce-scatter | all-reduce-scatter fusion | flops 32769 | bytes 131584
  76.3 1.3 collective-permute-start
  77.6 0.1 copy.36
  77.7 33.7 %all-reduce.1 = f32[56,2]{1,0:T(8,128)S(1)} all-reduce(f32[56,2]{1,0:T(8,128)S(1)} %copy.36), channel_id=3, replica_groups=mesh['sp'=8,'tp'=4] {'sp'}, use_global_device_ids=true, to_apply=%region_6.0.clone | all-reduce | flops 112 | bytes 896
  111.4 0.0 copy-done.8
  111.4 0.6 fusion.74
  112.7 0.1 broadcast_bitcast_fusion.1
  112.7 0.0 copy-done
  112.7 2.5 %copy.38 = bf16[512,2048]{1,0:T(8,128)(2,1)} copy(bf16[512,2048]{0,1:T(8,128)(2,1)S(1)} %copy-done) | data formatting | bytes 4194304 | tf_op jit(solution)/shard_map/dot_general | solution.py:23
  115.2 0.0 copy-start.2
  115.2 2.5 %fusion.20 = bf16[256,512]{1,0:T(8,128)(2,1)S(1)} fusion(bf16[2,2048,512]{2,1,0:T(8,128)(2,1)} %param.15, bf16[256,2048]{1,0:T(8,128)(2,1)S(1)} %copy-done.3, f32[2048]{0:T(1024)S(1)} %bitcast.115, f32[256]{0:T(256)S(1)} %add_rsqrt_fusion.4), kind=kOutput, calls=%fused_computation.24 | convolution fusion | flops 539099136 | bytes 3417088 | tf_op jit(solution)/shard_map/dot_general | solution.py:24
  117.7 0.0 copy-done.2
  117.7 1.6 multiply_reduce_fusion
  120.0 2.9 %copy.37 = bf16[512,2048]{1,0:T(8,128)(2,1)S(1)} copy(bf16[512,2048]{0,1:T(8,128)(2,1)} %get-tuple-element.6) | data formatting | bytes 4194304 | tf_op jit(solution)/shard_map/dot_general | solution.py:74
  122.9 0.0 collective-permute-done
  123.0 0.1 concatenate
  123.1 0.0 copy-start.5
  123.1 2.0 convolution_convert_fusion.1
  125.1 10.3 %psum.14 = bf16[7,2048]{1,0:T(8,128)(2,1)S(1)} all-reduce(bf16[7,2048]{1,0:T(8,128)(2,1)S(1)} %convolution_convert_fusion.1), channel_id=1, replica_groups=mesh['sp'=8,'tp'=4] {'tp'}, use_global_device_ids=true, to_apply=%region_7.0 | all-reduce | flops 14336 | bytes 57344 | tf_op jit(solution)/shard_map/psum | solution.py:92
  135.4 0.1 fusion.47
  135.5 0.7 multiply_reduce_fusion.2
  136.3 0.1 multiply_convert_fusion.4
  136.3 30.5 %all-gather.1 = bf16[8,7,512]{2,1,0:T(8,128)(2,1)S(1)} all-gather(bf16[1,7,512]{2,1,0:T(8,128)(2,1)S(1)} %bitcast.114), channel_id=1, replica_groups=mesh['sp'=8,'tp'=4] {'sp'}, dimensions={0}, use_global_device_ids=true | all-gather | bytes 64512 | tf_op jit(solution)/shard_map/all_gather | solution.py:77
  166.9 0.0 copy-done.5
  166.9 0.3 fusion.76
  167.2 0.2 convolution_bitcast_fusion
  167.4 19.9 %fusion.1 = f32[8,512]{1,0:T(8,128)S(1)} fusion(f32[56,512]{1,0:T(8,128)S(1)} %bitcast.106), kind=kCustom, calls=%all-reduce-scatter.1 | all-reduce-scatter fusion | flops 32769 | bytes 131584
  187.3 1.9 collective-permute-start.1
  189.2 0.1 copy.43
  189.3 33.1 %all-reduce.3 = f32[56,2]{1,0:T(8,128)S(1)} all-reduce(f32[56,2]{1,0:T(8,128)S(1)} %copy.43), channel_id=5, replica_groups=mesh['sp'=8,'tp'=4] {'sp'}, use_global_device_ids=true, to_apply=%region_13.0.clone | all-reduce | flops 112 | bytes 896
  222.4 0.1 broadcast_bitcast_fusion
  222.5 0.0 collective-permute-done.1
  222.5 0.1 concatenate.1
  222.6 2.0 convolution_convert_fusion
  224.6 10.3 %psum.15 = bf16[7,2048]{1,0:T(8,128)(2,1)S(1)} all-reduce(bf16[7,2048]{1,0:T(8,128)(2,1)S(1)} %convolution_convert_fusion), channel_id=1, replica_groups=mesh['sp'=8,'tp'=4] {'tp'}, use_global_device_ids=true, to_apply=%region_14.0 | all-reduce | flops 14336 | bytes 57344 | tf_op jit(solution)/shard_map/psum | solution.py:92
  234.9 0.6 fusion.50
  (19 shorter events, 0.2 us)
Async XLA Ops:
  6.2 2.5 %copy-start.3 = (bf16[256,2048]{1,0:T(8,128)(2,1)S(1)}, bf16[256,2048]{1,0:T(8,128)(2,1)}, u32[]{:S(2)}) copy-start(bf16[256,2048]{1,0:T(8,128)(2,1)} %param.10) | copy-start | bytes 3145732
  8.6 3.4 %copy-start.1 = (bf16[2,2048,512]{2,1,0:T(8,128)(2,1)S(1)}, bf16[2,2048,512]{2,1,0:T(8,128)(2,1)}, u32[]{:S(2)}) copy-start(bf16[2,2048,512]{2,1,0:T(8,128)(2,1)} %param.13) | copy-start | bytes 12582916
  14.3 3.0 %copy-start.7 = (f32[2,2048]{1,0:T(2,128)S(1)}, f32[2,2048]{1,0:T(2,128)}, u32[]{:S(2)}) copy-start(f32[2,2048]{1,0:T(2,128)} %param.11) | copy-start | bytes 49156
  14.3 3.0 %copy-start.4 = (bf16[7,2048]{1,0:T(8,128)(2,1)S(1)}, bf16[7,2048]{1,0:T(8,128)(2,1)}, u32[]{:S(2)}) copy-start(bf16[7,2048]{1,0:T(8,128)(2,1)} %param.9) | copy-start | bytes 86020
  17.3 33.4 %copy-start.9 = (f32[2,2]{1,0:T(2,128)S(1)}, f32[2,2]{1,0:T(2,128)}, u32[]{:S(2)}) copy-start(f32[2,2]{1,0:T(2,128)} %param.17) | copy-start | bytes 52
  50.7 2.5 %copy-start.6 = (f32[256,2,256]{0,2,1:T(8,128)S(1)}, f32[256,2,256]{0,2,1:T(8,128)}, u32[]{:S(2)}) copy-start(f32[256,2,256]{0,2,1:T(8,128)} %get-tuple-element.20) | copy-start | bytes 1572868
  50.7 60.7 %copy-start.8 = (u32[32]{0:T(128)S(1)}, u32[32]{0:T(128)}, u32[]{:S(2)}) copy-start(u32[32]{0:T(128)} %constant.31) | copy-start | bytes 388
  50.7 62.0 %copy-start = (bf16[512,2048]{0,1:T(8,128)(2,1)S(1)}, bf16[512,2048]{0,1:T(8,128)(2,1)}, u32[]{:S(2)}) copy-start(bf16[512,2048]{0,1:T(8,128)(2,1)} %get-tuple-element.8) | copy-start | bytes 6291460
  76.3 46.7 %collective-permute-start = (f32[7,512]{1,0:T(8,128)S(1)}, f32[7,512]{1,0:T(8,128)S(1)}, u32[]{:S(2)}, u32[]{:S(2)}) collective-permute-start(f32[7,512]{1,0:T(8,128)S(1)} %slice.56), channel_id=1, source_target_pairs={{0,4},{4,8},{8,12},{12,16},{16,20},{20,24},{24,28},{1,5},{5,9},{9,... | collective-permute-start | bytes 43016
  115.2 2.5 %copy-start.2 = (bf16[512,2048]{1,0:T(8,128)(2,1)S(1)}, bf16[512,2048]{1,0:T(8,128)(2,1)}, u32[]{:S(2)}) copy-start(bf16[512,2048]{1,0:T(8,128)(2,1)} %copy.38) | copy-start | bytes 6291460
  123.1 43.9 %copy-start.5 = (f32[256,2,256]{0,2,1:T(8,128)S(1)}, f32[256,2,256]{0,2,1:T(8,128)}, u32[]{:S(2)}) copy-start(f32[256,2,256]{0,2,1:T(8,128)} %get-tuple-element.18) | copy-start | bytes 1572868
  187.3 35.2 %collective-permute-start.1 = (f32[7,512]{1,0:T(8,128)S(1)}, f32[7,512]{1,0:T(8,128)S(1)}, u32[]{:S(2)}, u32[]{:S(2)}) collective-permute-start(f32[7,512]{1,0:T(8,128)S(1)} %slice.57), channel_id=1, source_target_pairs={{0,4},{4,8},{8,12},{12,16},{16,20},{20,24},{24,28},{1,5},{5,9},{9,... | collective-permute-start | bytes 43016
where the time goes:
time: 236 us; the launch traced here: 235 us
  blocking collectives  193 us (82%)
  local copies, waits for them, and re-layouts  19.1 us (8%)
  matrix products  16.3 us (7%)
  starting transfers between devices  3.19 us (1%)
  other arithmetic  2.62 us (1%)
    unnamed x4, blocking collectives  109 us
    all_gather x2, blocking collectives, body(): lax.all_gather(query_rows, 'sp', axis=0, tiled=True)  62.9 us
    psum x2, blocking collectives, body(): lax.psum(share.astype(jnp.float32).astype(jnp.bfloat16), 'tp')  20.5 us
    dot_general x3, local copies, waits for them, and re-layouts, source_side(): jnp.dot(normed_src, key_weight, preferred_element_type=jnp.float32)  8.79 us
    dot_general x3, local copies, waits for them, and re-layouts, body(): jnp.dot(normed_tgt, weight_now, preferred_element_type=jnp.float32)  8.14 us
    dot_general x2, matrix products, source_side(): jnp.dot(normed_src, key_weight, preferred_element_type=jnp.float32)  4.99 us
    dot_general x2, matrix products, source_side(): jnp.dot(normed_src, value_weight, preferred_element_type=jnp.float32)  4.98 us
  transfers between devices with their start and end apart: 2, of which 0 were waited for; matrix products, arithmetic and copies ran while one was open for 4% of the time, Pallas kernels for 0%

commit v1 on v0

--- a/solution.py
+++ b/solution.py
@@ -89,7 +89,9 @@
         share = jnp.dot(attended, w_out[layer_index], preferred_element_type=jnp.float32).astype(
             jnp.bfloat16
         )
-        branch = lax.psum(share.astype(jnp.float32).astype(jnp.bfloat16), "tp").astype(jnp.float32)
+        branch = jnp.sum(
+            lax.all_gather(share.astype(jnp.float32).astype(jnp.bfloat16), "tp"), axis=0
+        ).astype(jnp.float32)
         hidden = (hidden_float + branch).astype(jnp.bfloat16)
     return hidden
 

time: 236 us -> 226 us (0.958)
  blocking collectives: 193 us -> 183 us
    psum x2 -> x0, blocking collectives: 20.5 us -> none  [body(): lax.psum(share.astype(jnp.float32).astype(jnp.bfloat16), 'tp')]
    all_gather x0 -> x2, blocking collectives: none -> 10.8 us  [body(): lax.all_gather(share.astype(jnp.float32).astype(jnp.bfloat16), 'tp')]
  transfers between devices with their start and end apart: 2 -> 2, of which waited for: 0 -> 0; matrix products, arithmetic and copies ran while one was open for 4% -> 5% of each run, Pallas kernels for 0% -> 0%
where the time goes in v1:
time: 226 us
  blocking collectives  183 us (81%)
  local copies, waits for them, and re-layouts  19.1 us (8%)
  matrix products  16.3 us (7%)
  starting transfers between devices  3.15 us (1%)
  other arithmetic  2.68 us (1%)
    unnamed x4, blocking collectives  109 us
    all_gather x2, blocking collectives, body(): lax.all_gather(query_rows, 'sp', axis=0, tiled=True)  62.9 us
    all_gather x2, blocking collectives, body(): lax.all_gather(share.astype(jnp.float32).astype(jnp.bfloat16), 'tp')  10.8 us
    dot_general x3, local copies, waits for them, and re-layouts, source_side(): jnp.dot(normed_src, key_weight, preferred_element_type=jnp.float32)  8.79 us
    dot_general x3, local copies, waits for them, and re-layouts, body(): jnp.dot(normed_tgt, weight_now, preferred_element_type=jnp.float32)  8.14 us
    dot_general x2, matrix products, source_side(): jnp.dot(normed_src, key_weight, preferred_element_type=jnp.float32)  4.99 us
    dot_general x2, matrix products, source_side(): jnp.dot(normed_src, value_weight, preferred_element_type=jnp.float32)  4.98 us
  transfers between devices with their start and end apart: 2, of which 0 were waited for; matrix products, arithmetic and copies ran while one was open for 5% of the time, Pallas kernels for 0%

profile of v1, /device:TPU:0, one launch (start us, length us, event | category | flops | bytes accessed | tf_op | source)
XLA Modules:
  0.0 225.8 jit_solution(9364818347605474354)
XLA Ops:
  0.0 1.5 fusion.8
  1.5 0.8 fusion.75
  2.3 3.8 %slice_bitcast_fusion.2 = (bf16[512,2048]{0,1:T(8,128)(2,1)S(1)}, bf16[512,2048]{0,1:T(8,128)(2,1)}) fusion(bf16[2,2048,512]{2,1,0:T(8,128)(2,1)} %param.14), kind=kLoop, calls=%fused_computation.22 | loop fusion | bytes 8388608 | tf_op jit(solution)/shard_map/dot_general | solution.py:23
  6.2 0.0 copy-start.3
  6.2 2.5 %copy.31 = bf16[512,2048]{1,0:T(8,128)(2,1)} copy(bf16[512,2048]{0,1:T(8,128)(2,1)S(1)} %get-tuple-element.7) | data formatting | bytes 4194304 | tf_op jit(solution)/shard_map/dot_general | solution.py:23
  8.6 0.0 copy-done.3
  8.6 0.0 copy-start.1
  8.6 3.4 %multiply_reduce_fusion.1 = (f32[256,2]{0,1:T(2,128)S(1)}, f32[256,2,256]{0,2,1:T(8,128)}) fusion(bf16[2,256,2048]{2,1,0:T(8,128)(2,1)} %bitcast.108, f32[2048]{0:T(1024)S(1)} %bitcast.121, f32[256]{0:T(256)S(1)} %add_rsqrt_fusion.4, bf16[256,2048]{1,0:T(8,128)(2,1)S(1)} %copy-done.3), kind=kOutput, calls=%fused_computation.44 | convolution fusion | flops 539229696 | bytes 3681280 | tf_op jit(solution)/shard_map/dot_general | solution.py:23
  12.0 0.0 copy-done.1
  12.0 2.3 %slice_bitcast_fusion.3 = (bf16[512,2048]{0,1:T(8,128)(2,1)}, bf16[512,2048]{0,1:T(8,128)(2,1)}) fusion(bf16[2,2048,512]{2,1,0:T(8,128)(2,1)S(1)} %copy-done.1), kind=kLoop, calls=%fused_computation.23 | loop fusion | bytes 8388608 | tf_op jit(solution)/shard_map/dot_general | solution.py:74
  14.3 0.0 copy-start.7
  14.3 0.0 copy-start.4
  14.3 2.9 %copy.30 = bf16[512,2048]{1,0:T(8,128)(2,1)S(1)} copy(bf16[512,2048]{0,1:T(8,128)(2,1)} %get-tuple-element.5) | data formatting | bytes 4194304 | tf_op jit(solution)/shard_map/dot_general | solution.py:74
  17.3 0.0 copy-done.7
  17.3 0.0 copy-start.9
  17.3 0.0 copy-done.4
  17.3 0.1 fusion.45
  17.5 0.7 multiply_reduce_fusion.3
  18.2 0.1 multiply_convert_fusion.5
  18.3 32.4 %all-gather.2 = bf16[8,7,512]{2,1,0:T(8,128)(2,1)S(1)} all-gather(bf16[1,7,512]{2,1,0:T(8,128)(2,1)S(1)} %bitcast.117), channel_id=1, replica_groups=mesh['sp'=8,'tp'=4] {'sp'}, dimensions={0}, use_global_device_ids=true | all-gather | bytes 64512 | tf_op jit(solution)/shard_map/all_gather | solution.py:77
  50.7 0.0 copy-done.9
  50.7 0.0 copy-start.6
  50.7 0.0 copy-start.8
  50.7 0.0 copy-start
  50.7 2.5 %fusion.19 = bf16[256,512]{1,0:T(8,128)(2,1)S(1)} fusion(bf16[2,2048,512]{2,1,0:T(8,128)(2,1)} %param.15, bf16[256,2048]{1,0:T(8,128)(2,1)S(1)} %copy-done.3, f32[2048]{0:T(1024)S(1)} %bitcast.122, f32[256]{0:T(256)S(1)} %add_rsqrt_fusion.4), kind=kOutput, calls=%fused_computation.25 | convolution fusion | flops 539099136 | bytes 3417088 | tf_op jit(solution)/shard_map/dot_general | solution.py:24
  53.2 0.0 copy-done.6
  53.2 0.3 fusion.77
  53.5 0.2 convolution_bitcast_fusion.1
  53.7 22.6 %fusion = f32[8,512]{1,0:T(8,128)S(1)} fusion(f32[56,512]{1,0:T(8,128)S(1)} %bitcast.109), kind=kCustom, calls=%all-reduce-scatter | all-reduce-scatter fusion | flops 32769 | bytes 131584
  76.3 1.3 collective-permute-start
  77.6 0.1 copy.36
  77.7 33.7 %all-reduce.1 = f32[56,2]{1,0:T(8,128)S(1)} all-reduce(f32[56,2]{1,0:T(8,128)S(1)} %copy.36), channel_id=5, replica_groups=mesh['sp'=8,'tp'=4] {'sp'}, use_global_device_ids=true, to_apply=%region_6.0.clone | all-reduce | flops 112 | bytes 896
  111.4 0.0 copy-done.8
  111.4 0.6 fusion.76
  112.7 0.1 broadcast_bitcast_fusion.1
  112.7 0.0 copy-done
  112.7 2.5 %copy.38 = bf16[512,2048]{1,0:T(8,128)(2,1)} copy(bf16[512,2048]{0,1:T(8,128)(2,1)S(1)} %copy-done) | data formatting | bytes 4194304 | tf_op jit(solution)/shard_map/dot_general | solution.py:23
  115.2 0.0 copy-start.2
  115.2 2.5 %fusion.22 = bf16[256,512]{1,0:T(8,128)(2,1)S(1)} fusion(bf16[2,2048,512]{2,1,0:T(8,128)(2,1)} %param.15, bf16[256,2048]{1,0:T(8,128)(2,1)S(1)} %copy-done.3, f32[2048]{0:T(1024)S(1)} %bitcast.119, f32[256]{0:T(256)S(1)} %add_rsqrt_fusion.4), kind=kOutput, calls=%fused_computation.26 | convolution fusion | flops 539099136 | bytes 3417088 | tf_op jit(solution)/shard_map/dot_general | solution.py:24
  117.7 0.0 copy-done.2
  117.7 1.6 multiply_reduce_fusion
  120.0 2.9 %copy.37 = bf16[512,2048]{1,0:T(8,128)(2,1)S(1)} copy(bf16[512,2048]{0,1:T(8,128)(2,1)} %get-tuple-element.6) | data formatting | bytes 4194304 | tf_op jit(solution)/shard_map/dot_general | solution.py:74
  122.9 0.0 collective-permute-done
  123.0 0.1 concatenate
  123.1 0.0 copy-start.5
  123.1 2.0 fusion.4
  125.1 5.4 %all-gather.3 = bf16[4,7,2048]{2,1,0:T(8,128)(2,1)S(1)} all-gather(bf16[1,7,2048]{2,1,0:T(8,128)(2,1)S(1)} %fusion.4), channel_id=2, replica_groups=mesh['sp'=8,'tp'=4] {'tp'}, dimensions={0}, use_global_device_ids=true | all-gather | bytes 143360 | tf_op jit(solution)/shard_map/all_gather | solution.py:93
  130.6 0.1 fusion.49
  130.7 0.7 multiply_reduce_fusion.2
  131.4 0.1 multiply_convert_fusion.4
  131.5 30.5 %all-gather.4 = bf16[8,7,512]{2,1,0:T(8,128)(2,1)S(1)} all-gather(bf16[1,7,512]{2,1,0:T(8,128)(2,1)S(1)} %bitcast.118), channel_id=1, replica_groups=mesh['sp'=8,'tp'=4] {'sp'}, dimensions={0}, use_global_device_ids=true | all-gather | bytes 64512 | tf_op jit(solution)/shard_map/all_gather | solution.py:77
  162.1 0.0 copy-done.5
  162.1 0.3 fusion.78
  162.4 0.2 convolution_bitcast_fusion
  162.6 19.9 %fusion.1 = f32[8,512]{1,0:T(8,128)S(1)} fusion(f32[56,512]{1,0:T(8,128)S(1)} %bitcast.110), kind=kCustom, calls=%all-reduce-scatter.1 | all-reduce-scatter fusion | flops 32769 | bytes 131584
  182.5 1.9 collective-permute-start.1
  184.4 0.1 copy.43
  184.5 33.1 %all-reduce.3 = f32[56,2]{1,0:T(8,128)S(1)} all-reduce(f32[56,2]{1,0:T(8,128)S(1)} %copy.43), channel_id=7, replica_groups=mesh['sp'=8,'tp'=4] {'sp'}, use_global_device_ids=true, to_apply=%region_13.0.clone | all-reduce | flops 112 | bytes 896
  217.6 0.1 broadcast_bitcast_fusion
  217.7 0.0 collective-permute-done.1
  217.7 0.1 concatenate.1
  217.8 2.0 fusion.5
  219.8 5.4 %all-gather.5 = bf16[4,7,2048]{2,1,0:T(8,128)(2,1)S(1)} all-gather(bf16[1,7,2048]{2,1,0:T(8,128)(2,1)S(1)} %fusion.5), channel_id=3, replica_groups=mesh['sp'=8,'tp'=4] {'tp'}, dimensions={0}, use_global_device_ids=true | all-gather | bytes 143360 | tf_op jit(solution)/shard_map/all_gather | solution.py:93
  225.2 0.6 fusion.52
  (21 shorter events, 0.3 us)
Async XLA Ops:
  6.2 2.5 %copy-start.3 = (bf16[256,2048]{1,0:T(8,128)(2,1)S(1)}, bf16[256,2048]{1,0:T(8,128)(2,1)}, u32[]{:S(2)}) copy-start(bf16[256,2048]{1,0:T(8,128)(2,1)} %param.10) | copy-start | bytes 3145732
  8.6 3.4 %copy-start.1 = (bf16[2,2048,512]{2,1,0:T(8,128)(2,1)S(1)}, bf16[2,2048,512]{2,1,0:T(8,128)(2,1)}, u32[]{:S(2)}) copy-start(bf16[2,2048,512]{2,1,0:T(8,128)(2,1)} %param.13) | copy-start | bytes 12582916
  14.3 3.0 %copy-start.7 = (f32[2,2048]{1,0:T(2,128)S(1)}, f32[2,2048]{1,0:T(2,128)}, u32[]{:S(2)}) copy-start(f32[2,2048]{1,0:T(2,128)} %param.11) | copy-start | bytes 49156
  14.3 3.0 %copy-start.4 = (bf16[7,2048]{1,0:T(8,128)(2,1)S(1)}, bf16[7,2048]{1,0:T(8,128)(2,1)}, u32[]{:S(2)}) copy-start(bf16[7,2048]{1,0:T(8,128)(2,1)} %param.9) | copy-start | bytes 86020
  17.3 33.4 %copy-start.9 = (f32[2,2]{1,0:T(2,128)S(1)}, f32[2,2]{1,0:T(2,128)}, u32[]{:S(2)}) copy-start(f32[2,2]{1,0:T(2,128)} %param.17) | copy-start | bytes 52
  50.7 2.5 %copy-start.6 = (f32[256,2,256]{0,2,1:T(8,128)S(1)}, f32[256,2,256]{0,2,1:T(8,128)}, u32[]{:S(2)}) copy-start(f32[256,2,256]{0,2,1:T(8,128)} %get-tuple-element.20) | copy-start | bytes 1572868
  50.7 60.7 %copy-start.8 = (u32[32]{0:T(128)S(1)}, u32[32]{0:T(128)}, u32[]{:S(2)}) copy-start(u32[32]{0:T(128)} %constant.34) | copy-start | bytes 388
  50.7 62.0 %copy-start = (bf16[512,2048]{0,1:T(8,128)(2,1)S(1)}, bf16[512,2048]{0,1:T(8,128)(2,1)}, u32[]{:S(2)}) copy-start(bf16[512,2048]{0,1:T(8,128)(2,1)} %get-tuple-element.8) | copy-start | bytes 6291460
  76.3 46.7 %collective-permute-start = (f32[7,512]{1,0:T(8,128)S(1)}, f32[7,512]{1,0:T(8,128)S(1)}, u32[]{:S(2)}, u32[]{:S(2)}) collective-permute-start(f32[7,512]{1,0:T(8,128)S(1)} %slice.56), channel_id=1, source_target_pairs={{0,4},{4,8},{8,12},{12,16},{16,20},{20,24},{24,28},{1,5},{5,9},{9,... | collective-permute-start | bytes 43016
  115.2 2.5 %copy-start.2 = (bf16[512,2048]{1,0:T(8,128)(2,1)S(1)}, bf16[512,2048]{1,0:T(8,128)(2,1)}, u32[]{:S(2)}) copy-start(bf16[512,2048]{1,0:T(8,128)(2,1)} %copy.38) | copy-start | bytes 6291460
  123.1 39.0 %copy-start.5 = (f32[256,2,256]{0,2,1:T(8,128)S(1)}, f32[256,2,256]{0,2,1:T(8,128)}, u32[]{:S(2)}) copy-start(f32[256,2,256]{0,2,1:T(8,128)} %get-tuple-element.18) | copy-start | bytes 1572868
  182.5 35.1 %collective-permute-start.1 = (f32[7,512]{1,0:T(8,128)S(1)}, f32[7,512]{1,0:T(8,128)S(1)}, u32[]{:S(2)}, u32[]{:S(2)}) collective-permute-start(f32[7,512]{1,0:T(8,128)S(1)} %slice.57), channel_id=1, source_target_pairs={{0,4},{4,8},{8,12},{12,16},{16,20},{20,24},{24,28},{1,5},{5,9},{9,... | collective-permute-start | bytes 43016
